TPU v7x, 32 devices: a whole 2x2x4 slice. The times are simulated.
32 devices in a mesh: sp: 8 (over z, x), tp: 4 (over y, core).
Axes of the slice: x: 2, y: 2, z: 4, core: 2. Of those that a mesh axis runs over, the one named last changes fastest.
Arguments:
- residual: bfloat16 [2048, 2048], P(('sp', 'tp')), may hold values from -6 to 6
- query_wide: bfloat16 [2048, 512], P('sp', 'tp'), may hold values from -8 to 8
- key_wide: bfloat16 [2048, 512], P('sp', 'tp'), may hold values from -8 to 8
- value_wide: bfloat16 [2048, 512], P('sp', 'tp'), may hold values from -6 to 6
- query_narrow: bfloat16 [2048, 512], P('sp', 'tp'), may hold values from -8 to 8
- key_narrow: bfloat16 [2048, 512], P('sp', 'tp'), may hold values from -8 to 8
- value_narrow: bfloat16 [2048, 512], P('sp', 'tp'), may hold values from -6 to 6
- gate_wide: float32 [2048, 4], P('sp', 'tp'), may hold values from -2 to 20
- gate_narrow: float32 [2048, 8], P('sp', 'tp'), may hold values from -2 to 20
- out_wide: bfloat16 [512, 2048], replicated, may hold values from -0.1875 to 0.1875
- out_narrow: bfloat16 [512, 2048], replicated, may hold values from -0.1875 to 0.1875
- norm_gain: float32 [2048], replicated, may hold values from 0.1 to 1.9
- routing: int32 [2048, 2], P(('sp', 'tp')), may hold values from 0 to 7, as said below
- route_weight: float32 [2048, 2], P(('sp', 'tp')), may hold values from 0.3 to 1.5
- gate_weight: bfloat16 [8, 2048, 1024], P('sp', None, 'tp'), may hold values from -0.125 to 0.125
- up_weight: bfloat16 [8, 2048, 1024], P('sp', None, 'tp'), may hold values from -0.125 to 0.125
- down_weight: bfloat16 [8, 1024, 2048], P('sp', 'tp'), may hold values from -0.1875 to 0.1875
Outputs:
- result: bfloat16 [2048, 2048], P(('sp', 'tp'))
Inputs may be any that keep to these rules, and one draw needn't show every extreme that they name: `routing`: each row names 2 different experts of one group (experts g * 2 to g * 2 + 1). In each aligned block of 64 rows (the rows of one device) no expert is named by more than 32 rows; one group, the same for all blocks, has each of its experts named by exactly 32 rows of every block.
All inputs are finite; a program needn't handle non-finite values.
Results may differ from a plain program's by a relative error of at most 0.017.
Values may be sent and summed in bfloat16 or wider, within the bound.
A program may use at most 128 MiB of HBM per device.

v0:
```python
import math
import jax
import jax.numpy as jnp
from jax import lax
from jax.sharding import PartitionSpec as P

HW = 128
HN = 64
GROUPS = 4
epsilon = 1e-06


def globalize(pieces, shard_rows):
    shards = pieces.shape[0] // shard_rows
    grid = pieces.reshape(shards, shard_rows, pieces.shape[1])
    endings = grid[:, -1, :]
    offsets = jnp.cumsum(endings, axis=0) - endings
    return (grid + offsets[:, None, :]).reshape(pieces.shape)


def head_block(
    state, queries, query_decay, keys, values, key_decay, first_key, first_query, head_width
):
    highest_old, weight_sum, weighted = state
    query_rows = queries.shape[0]
    head_count = query_decay.shape[1]
    key_rows = keys.shape[0]
    grid_query = queries.reshape(query_rows, head_count, head_width)
    grid_key = keys.reshape(key_rows, head_count, head_width)
    grid_value = values.reshape(key_rows, head_count, head_width)
    scores = jnp.einsum("thd,phd->htp", grid_query, grid_key, preferred_element_type=jnp.float32)
    scores = scores * head_width ** (-0.5) + query_decay.T[:, :, None] - key_decay.T[:, None, :]
    query_place = first_query + jnp.arange(query_rows, dtype=jnp.int32)
    key_place = first_key + jnp.arange(key_rows, dtype=jnp.int32)
    scores = jnp.where(key_place[None, None, :] <= query_place[None, :, None], scores, -jnp.inf)
    highest = jnp.maximum(highest_old, jnp.max(scores, axis=2))
    weights = jnp.exp(scores - highest[:, :, None])
    shrink = jnp.exp(highest_old - highest)
    weight_sum = weight_sum * shrink + jnp.sum(weights, axis=2)
    product = jnp.einsum(
        "htp,phd->htd", weights.astype(jnp.bfloat16), grid_value, preferred_element_type=jnp.float32
    )
    weighted = weighted * shrink[:, :, None] + product
    return (highest, weight_sum, weighted)


def fresh_state(head_count, shard_rows, head_width):
    return (
        jnp.full((head_count, shard_rows), -1e30, jnp.float32),
        jnp.zeros((head_count, shard_rows), jnp.float32),
        jnp.zeros((head_count, shard_rows, head_width), jnp.float32),
    )


def finish(state, shard_rows):
    highest, weight_sum, weighted = state
    mixed_heads = weighted / weight_sum[:, :, None]
    joined = jnp.transpose(mixed_heads, (1, 0, 2))
    return joined.reshape(shard_rows, weighted.shape[0] * weighted.shape[2]).astype(jnp.bfloat16)


def body(
    residual,
    query_wide,
    key_wide,
    value_wide,
    query_narrow,
    key_narrow,
    value_narrow,
    gate_wide,
    gate_narrow,
    out_wide,
    out_narrow,
    norm_gain,
    routing,
    route_weight,
    gate_weight,
    up_weight,
    down_weight,
):
    shard_rows = query_wide.shape[0]
    half_rows = shard_rows // 2
    sp_place = lax.axis_index("sp")
    first_query = sp_place * shard_rows
    running_wide = jnp.cumsum(jax.nn.log_sigmoid(gate_wide), axis=0)
    running_narrow = jnp.cumsum(jax.nn.log_sigmoid(gate_narrow), axis=0)
    pieces_wide, pieces_narrow = (
        lax.all_gather(running_wide, "sp", axis=0, tiled=True),
        lax.all_gather(running_narrow, "sp", axis=0, tiled=True),
    )
    every_wide = globalize(pieces_wide, shard_rows)
    every_narrow = globalize(pieces_narrow, shard_rows)
    late_first = first_query + half_rows
    halves = []
    for place, part_wide, part_narrow in (
        (first_query, query_wide[:half_rows], query_narrow[:half_rows]),
        (late_first, query_wide[half_rows:], query_narrow[half_rows:]),
    ):
        halves.append(
            (
                place,
                part_wide,
                part_narrow,
                lax.dynamic_slice_in_dim(every_wide, place, half_rows, 0),
                lax.dynamic_slice_in_dim(every_narrow, place, half_rows, 0),
            )
        )

    def half_state():
        return (
            fresh_state(gate_wide.shape[1], half_rows, HW),
            fresh_state(gate_narrow.shape[1], half_rows, HN),
        )

    state = (half_state(), half_state())
    keys_wide = lax.all_gather(key_wide, "sp", axis=0, tiled=True)
    values_wide = lax.all_gather(value_wide, "sp", axis=0, tiled=True)
    keys_narrow = lax.all_gather(key_narrow, "sp", axis=0, tiled=True)
    values_narrow = lax.all_gather(value_narrow, "sp", axis=0, tiled=True)
    span_rows = keys_wide.shape[0]
    block_size = math.gcd(span_rows, 2048)

    def visit(carried, position):
        inside = position * block_size

        def take_block(source):
            return lax.dynamic_slice_in_dim(source, inside, block_size, 0)

        def take_decay(source):
            return lax.dynamic_slice_in_dim(source, inside, block_size, 0)

        block_kw = take_block(keys_wide)
        block_vw = take_block(values_wide)
        block_kn = take_block(keys_narrow)
        block_vn = take_block(values_narrow)
        block_dw = take_decay(every_wide)
        block_dn = take_decay(every_narrow)

        def one_half(current, half):
            place, part_wide, part_narrow, query_decay_wide, query_decay_narrow = half

            def work(inner):
                first = head_block(
                    inner[0],
                    part_wide,
                    query_decay_wide,
                    block_kw,
                    block_vw,
                    block_dw,
                    inside,
                    place,
                    HW,
                )
                second = head_block(
                    inner[1],
                    part_narrow,
                    query_decay_narrow,
                    block_kn,
                    block_vn,
                    block_dn,
                    inside,
                    place,
                    HN,
                )
                return (first, second)

            def skip(inner):
                return inner

            return lax.cond(inside <= place + half_rows - 1, work, skip, current)

        updated = (one_half(carried[0], halves[0]), one_half(carried[1], halves[1]))
        return (updated, None)

    state, _ = lax.scan(visit, state, jnp.arange(span_rows // block_size, dtype=jnp.int32))
    att_wide = jnp.concatenate(
        [finish(state[0][0], half_rows), finish(state[1][0], half_rows)], axis=0
    )
    att_narrow = jnp.concatenate(
        [finish(state[0][1], half_rows), finish(state[1][1], half_rows)], axis=0
    )
    own_rows = residual.shape[0]
    tp_place = lax.axis_index("tp")
    rows_wide = lax.dynamic_slice_in_dim(
        out_wide, tp_place * att_wide.shape[1], att_wide.shape[1], 0
    )
    rows_narrow = lax.dynamic_slice_in_dim(
        out_narrow, tp_place * att_narrow.shape[1], att_narrow.shape[1], 0
    )
    first = jnp.dot(att_wide, rows_wide, preferred_element_type=jnp.float32)
    second = jnp.dot(att_narrow, rows_narrow, preferred_element_type=jnp.float32)
    mixed = lax.psum_scatter(
        (first + second).astype(jnp.bfloat16), "tp", scatter_dimension=0, tiled=True
    ).astype(jnp.float32)
    middle = (residual.astype(jnp.float32) + mixed).astype(jnp.bfloat16)
    middle_wide = middle.astype(jnp.float32)
    spread = jnp.mean(middle_wide * middle_wide, axis=1, keepdims=True)
    normed = (middle_wide * lax.rsqrt(spread + epsilon) * norm_gain).astype(jnp.bfloat16)
    features = normed.shape[1]
    chosen_count = routing.shape[1]
    expert_count = gate_weight.shape[0] * lax.axis_size("sp")
    capacity = own_rows * GROUPS // expert_count
    flat_routes = routing.reshape(-1)
    matches = (flat_routes[:, None] == jnp.arange(expert_count, dtype=jnp.int32)[None, :]).astype(
        jnp.int32
    )
    ranking = jnp.sum((jnp.cumsum(matches, axis=0) - matches) * matches, axis=1)
    placing = flat_routes * capacity + ranking
    picker = (
        placing[None, :] == jnp.arange(expert_count * capacity, dtype=jnp.int32)[:, None]
    ).astype(jnp.bfloat16)
    picker = jnp.sum(picker.reshape(expert_count * capacity, own_rows, chosen_count), axis=2)
    outgoing = jnp.dot(picker, normed, preferred_element_type=jnp.float32).astype(jnp.bfloat16)
    outgoing = outgoing.reshape(expert_count, capacity, features)
    arrived = lax.all_to_all(outgoing, "sp", split_axis=0, concat_axis=0, tiled=True)
    pooled = lax.all_gather(arrived.reshape(-1, features), "tp", axis=0, tiled=True)
    gate_value = jnp.dot(pooled, gate_weight[0], preferred_element_type=jnp.float32)
    up_value = jnp.dot(pooled, up_weight[0], preferred_element_type=jnp.float32)
    hidden = (jax.nn.silu(gate_value) * up_value).astype(jnp.bfloat16)
    answers = lax.psum_scatter(
        jnp.dot(hidden, down_weight[0], preferred_element_type=jnp.float32).astype(jnp.bfloat16),
        "tp",
        scatter_dimension=0,
        tiled=True,
    )
    returned = lax.all_to_all(
        answers.reshape(expert_count, capacity, features),
        "sp",
        split_axis=0,
        concat_axis=0,
        tiled=True,
    )
    picked = jnp.take(returned.reshape(expert_count * capacity, features), placing, axis=0)
    picked = picked.reshape(own_rows, chosen_count, features).astype(jnp.float32)
    combined = jnp.sum(route_weight[:, :, None] * picked, axis=1)
    return (middle_wide + combined).astype(jnp.bfloat16)


def solution(mesh):
    placed = (
        P(("sp", "tp"), None),
        P("sp", "tp"),
        P("sp", "tp"),
        P("sp", "tp"),
        P("sp", "tp"),
        P("sp", "tp"),
        P("sp", "tp"),
        P("sp", "tp"),
        P("sp", "tp"),
        P(),
        P(),
        P(),
        P(("sp", "tp"), None),
        P(("sp", "tp"), None),
        P("sp", None, "tp"),
        P("sp", None, "tp"),
        P("sp", "tp", None),
    )
    return jax.shard_map(
        body, mesh=mesh, in_specs=placed, out_specs=P(("sp", "tp"), None), check_vma=False
    )
```

profile of v0, /device:TPU:0, one launch (start us, length us, event | category | flops | bytes accessed | tf_op | source)
XLA Modules:
  0.0 408.9 jit_solution(1248506105477989104)
XLA Ops:
  6.5 0.9 fusion.73
  7.4 0.6 reduce-window.16
  8.5 27.9 %all_gather.25 = f32[2048,2]{0,1:T(2,128)S(1)} all-gather(f32[256,2]{0,1:T(2,128)S(1)} %bitcast.168), channel_id=1, replica_groups=mesh['sp'=8,'tp'=4] {'sp'}, dimensions={0}, use_global_device_ids=true | all-gather | bytes 18432 | tf_op jit(solution)/shard_map/all_gather | solution.py:89
  36.9 0.7 fusion.74
  37.6 0.3 reduce-window.14
  37.9 0.2 slice_reduce_fusion.1
  38.3 19.0 %all_gather.22 = f32[2048,1]{0,1:T(1,128)S(1)} all-gather(f32[256,1]{0,1:T(1,128)S(1)} %reduce_window_sum.69), channel_id=1, replica_groups=mesh['sp'=8,'tp'=4] {'sp'}, dimensions={0}, use_global_device_ids=true | all-gather | bytes 9216 | tf_op jit(solution)/shard_map/all_gather | solution.py:88
  57.7 0.6 add.295
  58.3 0.9 copy.47
  59.3 33.5 %all_gather.24 = bf16[2048,128]{0,1:T(8,128)(2,1)} all-gather(bf16[256,128]{0,1:T(8,128)(2,1)S(1)} %copy.47), channel_id=1, replica_groups=mesh['sp'=8,'tp'=4] {'sp'}, dimensions={0}, use_global_device_ids=true | all-gather | bytes 589824 | tf_op jit(solution)/shard_map/all_gather | solution.py:118
  92.8 0.9 copy.49
  93.7 31.4 %all_gather.26 = bf16[2048,128]{0,1:T(8,128)(2,1)S(1)} all-gather(bf16[256,128]{0,1:T(8,128)(2,1)S(1)} %copy.49), channel_id=1, replica_groups=mesh['sp'=8,'tp'=4] {'sp'}, dimensions={0}, use_global_device_ids=true | all-gather | bytes 589824 | tf_op jit(solution)/shard_map/all_gather | solution.py:119
  125.1 33.7 %all_gather.21 = bf16[2048,128]{1,0:T(8,128)(2,1)} all-gather(bf16[256,128]{1,0:T(8,128)(2,1)} %param.23), channel_id=1, replica_groups=mesh['sp'=8,'tp'=4] {'sp'}, dimensions={0}, use_global_device_ids=true | all-gather | bytes 589824 | tf_op jit(solution)/shard_map/all_gather | solution.py:116
  158.9 31.2 %all_gather.23 = bf16[2048,128]{1,0:T(8,128)(2,1)S(1)} all-gather(bf16[256,128]{1,0:T(8,128)(2,1)S(1)} %copy-done.5), channel_id=1, replica_groups=mesh['sp'=8,'tp'=4] {'sp'}, dimensions={0}, use_global_device_ids=true | all-gather | bytes 589824 | tf_op jit(solution)/shard_map/all_gather | solution.py:117
  190.0 0.6 broadcast.260
  190.6 0.5 broadcast.258
  191.2 0.6 broadcast.265
  191.7 0.5 broadcast.263
  192.3 10.5 %conditional.3 = (f32[1,128]{1,0:T(1,128)S(1)}, f32[1,128,128]{2,1,0:T(8,128)S(1)}, f32[2,128]{1,0:T(2,128)}, f32[2,128,64]{1,2,0:T(8,128)}) conditional(s32[]{:T(128)} %convert_element_type.106, (f32[1,128]{1,0:T(1,128)}, f32[1,128,128]{2,1,0:T(8,128)S(1)}, f32[2,128]{1,0:T(2,128)}, f32[2,128,64]{1,2,0:T(8,128)S(1)}) %tuple.35, (s32[]{:T(128)}, ...), branch_computations={%region_12.13_spmd, %region_13.18_spmd.clone} | conditional | flops 276104320 | bytes 15037726 | solution.py:170
  192.3 0.7 dynamic-slice_bitcast_fusion.1
  192.9 0.6 copy-done.15
  193.5 0.2 iota_compare_fusion.1
  193.7 1.6 copy.51
  195.3 0.8 slice.51
  196.1 1.9 fusion.86
  198.0 0.4 fusion.26
  198.4 1.3 multiply_add_fusion.1
  199.7 1.2 convolution_add_fusion.1
  201.0 0.5 fusion.85
  201.5 0.4 fusion.27
  201.8 0.3 fusion.31
  202.1 0.6 bitcast_add_fusion.1
  202.8 0.5 copy-done.17
  203.3 8.7 %conditional.2 = ((f32[1,128]{1,0:T(1,128)}, f32[1,128,128]{2,1,0:T(8,128)S(1)}, f32[2,128]{1,0:T(2,128)}, f32[2,128,64]{1,2,0:T(8,128)S(1)})) conditional(s32[]{:T(128)} %convert_element_type.103, (f32[1,128]{1,0:T(1,128)}, f32[1,128,128]{2,1,0:T(8,128)S(1)}, f32[2,128]{1,0:T(2,128)}, f32[2,128,64]{1,2,0:T(8,128)S(1)}) %tuple.35, (s32[]{:T(128)}, ...), branch_computations={%region_6.7_spmd, %region_7.12_spmd.clone} | conditional | flops 276104320 | bytes 15033570 | solution.py:170
  203.4 0.9 iota_compare_fusion
  204.3 0.9 copy.50
  205.2 1.9 fusion.84
  207.2 0.4 fusion.7
  207.7 1.3 multiply_add_fusion
  208.9 0.6 convolution_add_fusion
  209.6 0.5 fusion.83
  210.1 0.4 fusion.8
  210.5 0.3 fusion.12
  210.8 1.2 bitcast_add_fusion
  211.9 0.7 divide_convert_fusion.1
  212.6 0.9 divide_convert_fusion
  213.5 0.7 fusion.70
  214.2 0.4 fusion.56
  214.7 2.5 fusion.38
  218.3 21.2 %reduce-scatter.3.cloned.1.call-done = bf16[64,2048]{1,0:T(8,128)(2,1)} async-done(((bf16[256,2048]{1,0:T(8,128)(2,1)}), bf16[64,2048]{1,0:T(8,128)(2,1)}) %reduce-scatter.3.cloned.1.call-update) | async-done | bytes 262160 | tf_op jit(solution)/shard_map/reduce_scatter | solution.py:192
  239.5 1.1 fusion.50
  240.7 1.4 convolution_convert_fusion.1
  242.2 31.1 %all_to_all.10 = bf16[8,32,2048]{2,1,0:T(8,128)(2,1)} all-to-all(bf16[8,32,2048]{2,1,0:T(8,128)(2,1)S(1)} %bitcast.150), channel_id=1, replica_groups=mesh['sp'=8,'tp'=4] {'sp'}, dimensions={0} | all-to-all | bytes 2097152 | tf_op jit(solution)/shard_map/all_to_all | solution.py:215
  273.3 0.2 reduce-scatter.5.cloned.1.call-start
  273.6 32.5 %all-gather.2.cloned.1.call-done = bf16[1024,2048]{1,0:T(8,128)(2,1)} async-done(((bf16[256,2048]{1,0:T(8,128)(2,1)}), bf16[1024,2048]{1,0:T(8,128)(2,1)}) %all-gather.2.cloned.1.call-update) | async-done | bytes 4194320 | tf_op jit(solution)/shard_map/all_gather | solution.py:216
  306.0 4.5 %fusion.43 = f32[1024,256]{1,0:T(8,128)} fusion(bf16[1024,2048]{1,0:T(8,128)(2,1)} %all-gather.2.cloned.1.call-done, bf16[1,2048,256]{2,1,0:T(8,128)(2,1)S(1)} %copy-done.18), kind=kOutput, calls=%fused_computation.73 | convolution fusion | flops 1073741824 | bytes 6291456 | tf_op jit(solution)/shard_map/dot_general | solution.py:217
  310.5 9.4 %convolution_convert_fusion = bf16[1024,2048]{1,0:T(8,128)(2,1)} fusion(bf16[1024,2048]{1,0:T(8,128)(2,1)} %all-gather.2.cloned.1.call-done, bf16[1,256,2048]{2,1,0:T(8,128)(2,1)} %param.37, bf16[1,2048,256]{2,1,0:T(8,128)(2,1)} %param.36, f32[1024,256]{1,0:T(8,128)} %fusion.43), kind=kOutput, calls=%fused_computation.65 | convolution fusion | flops 2151153664 | bytes 11534336 | tf_op jit(solution)/shard_map/dot_general | solution.py:221
  320.0 44.7 %reduce-scatter.5.cloned.1.call-done = bf16[256,2048]{1,0:T(8,128)(2,1)} async-done(((bf16[1024,2048]{1,0:T(8,128)(2,1)}), bf16[256,2048]{1,0:T(8,128)(2,1)}) %reduce-scatter.5.cloned.1.call-update) | async-done | bytes 1048592 | tf_op jit(solution)/shard_map/reduce_scatter | solution.py:220
  364.7 5.5 %all-to-all-start.1 = ((bf16[8,32,2048]{2,1,0:T(8,128)(2,1)}), bf16[8,32,2048]{2,1,0:T(8,128)(2,1)S(1)}, u32[]{:S(2)}, u32[]{:S(2)}) async-start(bf16[8,32,2048]{2,1,0:T(8,128)(2,1)} %bitcast.151), calls=%async_computation.3 | async-start | bytes 2097152 | tf_op jit(solution)/shard_map/all_to_all | solution.py:226
  370.7 25.2 %all-to-all-done.1 = bf16[8,32,2048]{2,1,0:T(8,128)(2,1)S(1)} async-done(((bf16[8,32,2048]{2,1,0:T(8,128)(2,1)}), bf16[8,32,2048]{2,1,0:T(8,128)(2,1)S(1)}, u32[]{:S(2)}, u32[]{:S(2)}) %all-to-all-start.1) | async-done | bytes 1048608 | tf_op jit(solution)/shard_map/all_to_all | solution.py:226
  395.9 1.7 gather_fusion
  397.6 1.4 gather.7
  399.0 2.5 multiply_reduce_fusion
  401.6 0.8 fusion.53
  (98 shorter events, 3.5 us)
Async XLA Ops:
  6.5 207.7 %copy-start = (bf16[512,2048]{1,0:T(8,128)(2,1)S(1)}, bf16[512,2048]{1,0:T(8,128)(2,1)}, u32[]{:S(2)}) copy-start(bf16[512,2048]{1,0:T(8,128)(2,1)} %param.30) | copy-start | bytes 6291460
  6.5 152.3 %copy-start.5 = (bf16[256,128]{1,0:T(8,128)(2,1)S(1)}, bf16[256,128]{1,0:T(8,128)(2,1)}, u32[]{:S(2)}) copy-start(bf16[256,128]{1,0:T(8,128)(2,1)} %param.24) | copy-start | bytes 196612
  6.5 233.0 %reduce-scatter.3.cloned.1.call-start = ((), (), s32[]{:S(2)}) async-start(), calls=%async_computation.4 | async-start | bytes 1310720 | tf_op jit(solution)/shard_map/reduce_scatter | solution.py:192
  192.9 0.6 copy-start.15
  195.3 2.6 copy-start.6
  198.0 2.9 copy-start.10
  198.0 3.0 copy-start.3
  198.0 3.0 copy-start.16
  198.0 3.0 copy-start.19
  199.7 1.8 copy-start.12
  202.8 0.5 copy-start.17
  203.4 3.8 copy-start.7
  207.2 2.3 copy-start.11
  207.2 2.4 copy-start.4
  207.2 2.4 copy-start.20
  208.9 1.2 copy-start.13
  214.7 2.7 copy-start.8
  214.7 24.9 %copy-start.1 = (bf16[64,2048]{1,0:T(8,128)(2,1)S(1)}, bf16[64,2048]{1,0:T(8,128)(2,1)}, u32[]{:S(2)}) copy-start(bf16[64,2048]{1,0:T(8,128)(2,1)} %param.21) | copy-start | bytes 786436
  214.7 26.0 %copy-start.9 = (f32[2048]{0:T(1024)S(1)}, f32[2048]{0:T(1024)}, u32[]{:S(2)}) copy-start(f32[2048]{0:T(1024)} %param.32) | copy-start | bytes 24580
  217.3 88.8 %all-gather.2.cloned.1.call-start = ((), (), s32[]{:S(2)}) async-start(), calls=%async_computation.5 | async-start | bytes 5242880 | tf_op jit(solution)/shard_map/all_gather | solution.py:216
  242.1 63.9 %copy-start.18 = (bf16[1,2048,256]{2,1,0:T(8,128)(2,1)S(1)}, bf16[1,2048,256]{2,1,0:T(8,128)(2,1)}, u32[]{:S(2)}) copy-start(bf16[1,2048,256]{2,1,0:T(8,128)(2,1)} %param.35) | copy-start | bytes 3145732
  273.3 91.4 %reduce-scatter.5.cloned.1.call-start = ((), (), s32[]{:S(2)}) async-start(), calls=%async_computation.6 | async-start | bytes 5242880 | tf_op jit(solution)/shard_map/reduce_scatter | solution.py:220
  320.0 50.6 %copy-start.14 = (f32[64,2]{0,1:T(2,128)S(1)}, f32[64,2]{0,1:T(2,128)}, u32[]{:S(2)}) copy-start(f32[64,2]{0,1:T(2,128)} %param.34) | copy-start | bytes 1540
  364.7 31.2 %all-to-all-start.1 = ((bf16[8,32,2048]{2,1,0:T(8,128)(2,1)}), bf16[8,32,2048]{2,1,0:T(8,128)(2,1)S(1)}, u32[]{:S(2)}, u32[]{:S(2)}) async-start(bf16[8,32,2048]{2,1,0:T(8,128)(2,1)} %bitcast.151), calls=%async_computation.3 | async-start | bytes 2097152 | tf_op jit(solution)/shard_map/all_to_all | solution.py:226
  397.6 4.0 copy-start.2
Sparse Core Ops, SparseCore 0:
  217.4 22.1 reduce-scatter.2
  273.5 32.5 all-gather.1
  320.1 44.5 reduce-scatter.4
where the time goes:
time: 410 us; the launch traced here: 409 us
  blocking collectives  208 us (51%)
  waiting for transfers between devices  124 us (30%)
  matrix products  25.6 us (6%)
  other arithmetic  18.2 us (4%)
  local copies, waits for them, and re-layouts  14.4 us (4%)
  between operations  13.4 us (3%)
  starting transfers between devices  5.77 us (1%)
    reduce_scatter x1, waiting for transfers between devices, body(): lax.psum_scatter(jnp.dot(hidden, down_weight[0], preferred_element_type=j...  44.7 us
    all_gather x1, blocking collectives, body(): keys_wide = lax.all_gather(key_wide, 'sp', axis=0, tiled=True)  33.7 us
    all_gather x1, blocking collectives, body(): keys_narrow = lax.all_gather(key_narrow, 'sp', axis=0, tiled=True)  33.5 us
    all_gather x1, waiting for transfers between devices, body(): lax.all_gather(arrived.reshape(-1, features), 'tp', axis=0, tiled=True)  32.5 us
    all_gather x1, blocking collectives, body(): values_narrow = lax.all_gather(value_narrow, 'sp', axis=0, tiled=True)  31.4 us
    all_gather x1, blocking collectives, body(): values_wide = lax.all_gather(value_wide, 'sp', axis=0, tiled=True)  31.2 us
    all_to_all x1, blocking collectives, body(): lax.all_to_all(outgoing, 'sp', split_axis=0, concat_axis=0, tiled=True)  31.1 us
    all_gather x1, blocking collectives, body(): lax.all_gather(running_narrow, 'sp', axis=0, tiled=True)  27.9 us
  transfers between devices with their start and end apart: 4, of which 4 were waited for; matrix products, arithmetic and copies ran while one was open for 0% of the time, Pallas kernels for 0%

commit v1 on v0

--- a/solution.py
+++ b/solution.py
@@ -3,6 +3,7 @@
 import jax.numpy as jnp
 from jax import lax
 from jax.sharding import PartitionSpec as P
+from jax.lax import all_gather
 
 HW = 128
 HN = 64
@@ -114,8 +115,13 @@
 
     state = (half_state(), half_state())
     keys_wide = lax.all_gather(key_wide, "sp", axis=0, tiled=True)
-    values_wide = lax.all_gather(value_wide, "sp", axis=0, tiled=True)
-    keys_narrow = lax.all_gather(key_narrow, "sp", axis=0, tiled=True)
+    values_wide, keys_narrow = jnp.split(
+        all_gather(
+            jnp.concatenate([value_wide, key_narrow], 1), axis_name="sp", axis=0, tiled=True
+        ),
+        [value_wide.shape[1]],
+        1,
+    )
     values_narrow = lax.all_gather(value_narrow, "sp", axis=0, tiled=True)
     span_rows = keys_wide.shape[0]
     block_size = math.gcd(span_rows, 2048)

time: 410 us -> 349 us (0.85)
  blocking collectives: 208 us -> 143 us
    all_gather x2 -> x0, blocking collectives: 64.7 us -> none  [the longest x1 33.5 us: body(): keys_narrow = lax.all_gather(key_narrow, 'sp', axis=0, tiled=True)]
  transfers between devices with their start and end apart: 4 -> 5, of which waited for: 4 -> 4; matrix products, arithmetic and copies ran while one was open for 0% -> 2% of each run, Pallas kernels for 0% -> 0%
where the time goes in v1:
time: 349 us; the launch traced here: 348 us
  blocking collectives  143 us (41%)
  waiting for transfers between devices  124 us (36%)
  matrix products  25.6 us (7%)
  other arithmetic  18.8 us (5%)
  local copies, waits for them, and re-layouts  17.7 us (5%)
  between operations  13.4 us (4%)
  starting transfers between devices  5.82 us (2%)
    reduce_scatter x1, waiting for transfers between devices, body(): lax.psum_scatter(jnp.dot(hidden, down_weight[0], preferred_element_type=j...  44.7 us
    all_gather x1, blocking collectives, body(): keys_wide = lax.all_gather(key_wide, 'sp', axis=0, tiled=True)  33.5 us
    all_gather x1, waiting for transfers between devices, body(): lax.all_gather(arrived.reshape(-1, features), 'tp', axis=0, tiled=True)  32.5 us
    all_gather x1, blocking collectives, body(): values_narrow = lax.all_gather(value_narrow, 'sp', axis=0, tiled=True)  31.5 us
    all_to_all x1, blocking collectives, body(): lax.all_to_all(outgoing, 'sp', split_axis=0, concat_axis=0, tiled=True)  31.1 us
    all_gather x1, blocking collectives, body(): lax.all_gather(running_narrow, 'sp', axis=0, tiled=True)  28 us
    all_to_all x1, waiting for transfers between devices, body(): lax.all_to_all(answers.reshape(expert_count, capacity, features), 'sp', s...  25.2 us
    reduce_scatter x1, waiting for transfers between devices, body(): lax.psum_scatter((first + second).astype(jnp.bfloat16), 'tp', scatter_dim...  21.2 us
  transfers between devices with their start and end apart: 5, of which 4 were waited for; matrix products, arithmetic and copies ran while one was open for 2% of the time, Pallas kernels for 0%

profile of v1, /device:TPU:0, one launch (start us, length us, event | category | flops | bytes accessed | tf_op | source)
XLA Modules:
  0.0 348.2 jit_solution(2062480744564855352)
XLA Ops:
  6.5 1.1 copy.56
  7.6 0.9 copy.57
  8.6 0.7 pad_maximum_fusion
  9.3 0.7 fusion.73
  10.0 0.6 reduce-window.16
  11.1 28.0 %all_gather.21 = f32[2048,2]{0,1:T(2,128)S(1)} all-gather(f32[256,2]{0,1:T(2,128)S(1)} %bitcast.168), channel_id=1, replica_groups=mesh['sp'=8,'tp'=4] {'sp'}, dimensions={0}, use_global_device_ids=true | all-gather | bytes 18432 | tf_op jit(solution)/shard_map/all_gather | solution.py:90
  39.5 0.7 fusion.74
  40.2 0.3 reduce-window.14
  41.0 19.1 %all_gather.19 = f32[2048,1]{0,1:T(1,128)S(1)} all-gather(f32[256,1]{0,1:T(1,128)S(1)} %reduce_window_sum.69), channel_id=1, replica_groups=mesh['sp'=8,'tp'=4] {'sp'}, dimensions={0}, use_global_device_ids=true | all-gather | bytes 9216 | tf_op jit(solution)/shard_map/all_gather | solution.py:89
  60.5 0.6 add.295
  61.1 0.9 copy.59
  62.1 0.6 broadcast.260
  62.7 0.6 broadcast.258
  63.2 31.5 %all_gather.22 = bf16[2048,128]{0,1:T(8,128)(2,1)S(1)} all-gather(bf16[256,128]{0,1:T(8,128)(2,1)S(1)} %copy.59), channel_id=1, replica_groups=mesh['sp'=8,'tp'=4] {'sp'}, dimensions={0}, use_global_device_ids=true | all-gather | bytes 589824 | tf_op jit(solution)/shard_map/all_gather | solution.py:125
  94.8 33.5 %all_gather.18 = bf16[2048,128]{1,0:T(8,128)(2,1)} all-gather(bf16[256,128]{1,0:T(8,128)(2,1)} %param.23), channel_id=1, replica_groups=mesh['sp'=8,'tp'=4] {'sp'}, dimensions={0}, use_global_device_ids=true | all-gather | bytes 589824 | tf_op jit(solution)/shard_map/all_gather | solution.py:117
  128.2 2.1 fusion.87
  130.3 0.5 broadcast.265
  130.9 0.5 broadcast.263
  131.4 10.5 %conditional.3 = (f32[1,128]{1,0:T(1,128)S(1)}, f32[1,128,128]{2,1,0:T(8,128)S(1)}, f32[2,128]{1,0:T(2,128)}, f32[2,128,64]{1,2,0:T(8,128)}) conditional(s32[]{:T(128)} %convert_element_type.106, (f32[1,128]{1,0:T(1,128)}, f32[1,128,128]{2,1,0:T(8,128)S(1)}, f32[2,128]{1,0:T(2,128)}, f32[2,128,64]{1,2,0:T(8,128)S(1)}) %tuple.35, (s32[]{:T(128)}, ...), branch_computations={%region_12.13_spmd, %region_13.18_spmd.clone} | conditional | flops 276104320 | bytes 15037726 | solution.py:176
  131.4 0.7 dynamic-slice_bitcast_fusion.1
  132.1 0.6 copy-done.14
  132.6 0.2 iota_compare_fusion.1
  132.9 1.6 copy.63
  134.4 0.8 slice.51
  135.2 1.9 fusion.86
  137.1 0.4 fusion.26
  137.6 1.2 multiply_add_fusion.1
  138.8 1.2 convolution_add_fusion.1
  140.1 0.5 fusion.85
  140.6 0.4 fusion.27
  141.0 0.3 fusion.31
  141.2 0.7 bitcast_add_fusion.1
  141.9 0.6 copy-done.16
  142.5 8.7 %conditional.2 = ((f32[1,128]{1,0:T(1,128)}, f32[1,128,128]{2,1,0:T(8,128)S(1)}, f32[2,128]{1,0:T(2,128)}, f32[2,128,64]{1,2,0:T(8,128)S(1)})) conditional(s32[]{:T(128)} %convert_element_type.103, (f32[1,128]{1,0:T(1,128)}, f32[1,128,128]{2,1,0:T(8,128)S(1)}, f32[2,128]{1,0:T(2,128)}, f32[2,128,64]{1,2,0:T(8,128)S(1)}) %tuple.35, (s32[]{:T(128)}, ...), branch_computations={%region_6.7_spmd, %region_7.12_spmd.clone} | conditional | flops 276104320 | bytes 15033570 | solution.py:176
  142.6 0.9 iota_compare_fusion
  143.5 0.9 copy.61
  144.5 1.9 fusion.84
  146.5 0.4 fusion.7
  146.9 1.3 multiply_add_fusion
  148.1 0.6 convolution_add_fusion
  148.8 0.5 fusion.83
  149.3 0.4 fusion.8
  149.7 0.3 fusion.12
  150.0 1.2 bitcast_add_fusion
  151.2 0.7 divide_convert_fusion.1
  151.9 0.9 divide_convert_fusion
  152.8 0.8 fusion.70
  153.6 0.4 fusion.56
  154.1 2.5 fusion.38
  157.7 21.2 %reduce-scatter.3.cloned.1.call-done = bf16[64,2048]{1,0:T(8,128)(2,1)} async-done(((bf16[256,2048]{1,0:T(8,128)(2,1)}), bf16[64,2048]{1,0:T(8,128)(2,1)}) %reduce-scatter.3.cloned.1.call-update) | async-done | bytes 262160 | tf_op jit(solution)/shard_map/reduce_scatter | solution.py:198
  178.9 1.1 fusion.50
  180.0 1.4 convolution_convert_fusion.1
  181.5 31.1 %all_to_all.10 = bf16[8,32,2048]{2,1,0:T(8,128)(2,1)} all-to-all(bf16[8,32,2048]{2,1,0:T(8,128)(2,1)S(1)} %bitcast.150), channel_id=1, replica_groups=mesh['sp'=8,'tp'=4] {'sp'}, dimensions={0} | all-to-all | bytes 2097152 | tf_op jit(solution)/shard_map/all_to_all | solution.py:221
  212.6 0.2 reduce-scatter.5.cloned.1.call-start
  212.9 32.5 %all-gather.5.cloned.1.call-done = bf16[1024,2048]{1,0:T(8,128)(2,1)} async-done(((bf16[256,2048]{1,0:T(8,128)(2,1)}), bf16[1024,2048]{1,0:T(8,128)(2,1)}) %all-gather.5.cloned.1.call-update) | async-done | bytes 4194320 | tf_op jit(solution)/shard_map/all_gather | solution.py:222
  245.3 4.5 %fusion.43 = f32[1024,256]{1,0:T(8,128)} fusion(bf16[1024,2048]{1,0:T(8,128)(2,1)} %all-gather.5.cloned.1.call-done, bf16[1,2048,256]{2,1,0:T(8,128)(2,1)S(1)} %copy-done.17), kind=kOutput, calls=%fused_computation.73 | convolution fusion | flops 1073741824 | bytes 6291456 | tf_op jit(solution)/shard_map/dot_general | solution.py:223
  249.8 9.4 %convolution_convert_fusion = bf16[1024,2048]{1,0:T(8,128)(2,1)} fusion(bf16[1024,2048]{1,0:T(8,128)(2,1)} %all-gather.5.cloned.1.call-done, bf16[1,256,2048]{2,1,0:T(8,128)(2,1)} %param.37, bf16[1,2048,256]{2,1,0:T(8,128)(2,1)} %param.36, f32[1024,256]{1,0:T(8,128)} %fusion.43), kind=kOutput, calls=%fused_computation.65 | convolution fusion | flops 2151153664 | bytes 11534336 | tf_op jit(solution)/shard_map/dot_general | solution.py:227
  259.3 44.7 %reduce-scatter.5.cloned.1.call-done = bf16[256,2048]{1,0:T(8,128)(2,1)} async-done(((bf16[1024,2048]{1,0:T(8,128)(2,1)}), bf16[256,2048]{1,0:T(8,128)(2,1)}) %reduce-scatter.5.cloned.1.call-update) | async-done | bytes 1048592 | tf_op jit(solution)/shard_map/reduce_scatter | solution.py:226
  304.0 5.5 %all-to-all-start.1 = ((bf16[8,32,2048]{2,1,0:T(8,128)(2,1)}), bf16[8,32,2048]{2,1,0:T(8,128)(2,1)S(1)}, u32[]{:S(2)}, u32[]{:S(2)}) async-start(bf16[8,32,2048]{2,1,0:T(8,128)(2,1)} %bitcast.151), calls=%async_computation.3 | async-start | bytes 2097152 | tf_op jit(solution)/shard_map/all_to_all | solution.py:232
  310.0 25.2 %all-to-all-done.1 = bf16[8,32,2048]{2,1,0:T(8,128)(2,1)S(1)} async-done(((bf16[8,32,2048]{2,1,0:T(8,128)(2,1)}), bf16[8,32,2048]{2,1,0:T(8,128)(2,1)S(1)}, u32[]{:S(2)}, u32[]{:S(2)}) %all-to-all-start.1) | async-done | bytes 1048608 | tf_op jit(solution)/shard_map/all_to_all | solution.py:232
  335.2 1.7 gather_fusion
  336.9 1.4 gather.7
  338.3 2.5 multiply_reduce_fusion
  340.9 0.8 fusion.53
  (100 shorter events, 3.7 us)
Async XLA Ops:
  6.5 147.0 %copy-start = (bf16[512,2048]{1,0:T(8,128)(2,1)S(1)}, bf16[512,2048]{1,0:T(8,128)(2,1)}, u32[]{:S(2)}) copy-start(bf16[512,2048]{1,0:T(8,128)(2,1)} %param.30) | copy-start | bytes 6291460
  6.5 121.7 %all-gather.3.cloned.1.call-start = ((), (), s32[]{:S(2)}) async-start(), calls=%async_computation.4 | async-start | bytes 1179648 | tf_op jit(solution)/shard_map/all_gather | solution.py:119
  9.3 169.6 %reduce-scatter.3.cloned.1.call-start = ((), (), s32[]{:S(2)}) async-start(), calls=%async_computation.5 | async-start | bytes 1310720 | tf_op jit(solution)/shard_map/reduce_scatter | solution.py:198
  132.1 0.6 copy-start.14
  134.4 2.6 copy-start.5
  137.1 2.9 copy-start.9
  137.1 3.0 copy-start.3
  137.1 3.0 copy-start.15
  137.1 3.0 copy-start.18
  138.8 1.8 copy-start.11
  141.9 0.6 copy-start.16
  142.6 3.8 %copy-start.6 = (f32[2,128]{1,0:T(2,128)S(1)}, f32[2,128]{1,0:T(2,128)}, u32[]{:S(2)}) copy-start(f32[2,128]{1,0:T(2,128)} %get-tuple-element.417) | copy-start | bytes 3076 | tf_op jit(solution)/shard_map/while/body/eval_jaxpr/cond
  146.4 2.3 copy-start.10
  146.4 2.4 copy-start.4
  146.4 2.4 copy-start.19
  148.1 1.2 copy-start.12
  154.0 2.7 copy-start.7
  154.0 24.8 %copy-start.1 = (bf16[64,2048]{1,0:T(8,128)(2,1)S(1)}, bf16[64,2048]{1,0:T(8,128)(2,1)}, u32[]{:S(2)}) copy-start(bf16[64,2048]{1,0:T(8,128)(2,1)} %param.21) | copy-start | bytes 786436
  154.0 26.0 %copy-start.8 = (f32[2048]{0:T(1024)S(1)}, f32[2048]{0:T(1024)}, u32[]{:S(2)}) copy-start(f32[2048]{0:T(1024)} %param.32) | copy-start | bytes 24580
  156.6 88.7 %all-gather.5.cloned.1.call-start = ((), (), s32[]{:S(2)}) async-start(), calls=%async_computation.6 | async-start | bytes 5242880 | tf_op jit(solution)/shard_map/all_gather | solution.py:222
  181.5 63.9 %copy-start.17 = (bf16[1,2048,256]{2,1,0:T(8,128)(2,1)S(1)}, bf16[1,2048,256]{2,1,0:T(8,128)(2,1)}, u32[]{:S(2)}) copy-start(bf16[1,2048,256]{2,1,0:T(8,128)(2,1)} %param.35) | copy-start | bytes 3145732
  212.6 91.4 %reduce-scatter.5.cloned.1.call-start = ((), (), s32[]{:S(2)}) async-start(), calls=%async_computation.7 | async-start | bytes 5242880 | tf_op jit(solution)/shard_map/reduce_scatter | solution.py:226
  259.3 50.6 %copy-start.13 = (f32[64,2]{0,1:T(2,128)S(1)}, f32[64,2]{0,1:T(2,128)}, u32[]{:S(2)}) copy-start(f32[64,2]{0,1:T(2,128)} %param.34) | copy-start | bytes 1540
  304.0 31.2 %all-to-all-start.1 = ((bf16[8,32,2048]{2,1,0:T(8,128)(2,1)}), bf16[8,32,2048]{2,1,0:T(8,128)(2,1)S(1)}, u32[]{:S(2)}, u32[]{:S(2)}) async-start(bf16[8,32,2048]{2,1,0:T(8,128)(2,1)} %bitcast.151), calls=%async_computation.3 | async-start | bytes 2097152 | tf_op jit(solution)/shard_map/all_to_all | solution.py:232
  336.9 4.0 %copy-start.2 = (bf16[64,2048]{1,0:T(8,128)(2,1)S(1)}, bf16[64,2048]{1,0:T(8,128)(2,1)}, u32[]{:S(2)}) copy-start(bf16[64,2048]{1,0:T(8,128)(2,1)} %reduce-scatter.3.cloned.1.call-done) | copy-start | bytes 786436
Sparse Core Ops, SparseCore 0:
  9.4 42.1 all-gather.2
  156.7 22.0 reduce-scatter.2
  212.8 32.5 all-gather.4
  259.4 44.5 reduce-scatter.4
